TPU v7x, 256 devices: a whole 4x4x8 slice. The times are simulated.
256 devices in a mesh: ra: 32 (over z, y), cb: 8 (over x, core).
Axes of the slice: x: 4, y: 4, z: 8, core: 2. Of those that a mesh axis runs over, the one named last changes fastest.
Arguments:
- tokens: bfloat16 [2048, 16384], P('ra'), may hold values from -16 to 16
- norm_gain: float32 [2, 2048], replicated, may hold values from 0.1 to 1.9
- up_weight: float32 [2, 2048, 6144], P(None, 'ra', 'cb'), may hold values from -0.125 to 0.125
- gate_weight: float32 [2, 2048, 6144], P(None, 'ra', 'cb'), may hold values from -0.125 to 0.125
- up_scale: float32 [2, 6144], P(None, 'cb'), may hold values from 0.5 to 2
- gate_scale: float32 [2, 6144], P(None, 'cb'), may hold values from 0.5 to 2
- up_taps: float32 [2, 3, 6144], P(None, None, 'cb'), may hold values from -3 to 3
- gate_taps: float32 [2, 3, 6144], P(None, None, 'cb'), may hold values from -3 to 3
- down_weight: float32 [2, 2048, 6144], P(None, 'ra', 'cb'), may hold values from -0.078125 to 0.078125
- down_scale: float32 [2, 2048], replicated, may hold values from 0.5 to 2
Outputs:
- mixed: bfloat16 [2048, 16384], P('ra')
All inputs are finite; a program needn't handle non-finite values.
Results may differ from a plain program's by a relative error of at most 0.024.
Values may be sent and summed in bfloat16 or wider, within the bound.
No kernel may reach another device: no remote copies, remote signals or barrier semaphores. Data moves between devices by JAX's collectives and lax.ppermute only.
A program may use at most 64 MiB of HBM per device.

v0:
```python
import jax
import jax.numpy as jnp
from jax import lax
from jax.sharding import Mesh
from jax.sharding import PartitionSpec as P

RA = ("z", "y")
CB = ("x", "c")
EPS = 1e-06
RESIDUAL = 0.5
BF = jnp.bfloat16
F32 = jnp.float32


def turned(value, axis, steps):
    count = lax.axis_size(axis)
    return lax.ppermute(value, axis, [(s, (s + steps) % count) for s in range(count)])


def shifted(value, axis, steps):
    count = lax.axis_size(axis)
    initial, last = (max(0, -steps), min(count, count - steps))
    return lax.ppermute(value, axis, [(s, s + steps) for s in range(initial, last)])


def at(blocks, index):
    return lax.dynamic_index_in_dim(blocks, index, 0, keepdims=False)


def gather_cb(own):
    half = own.shape[0] // 2
    x = lax.axis_index("x")
    c = lax.axis_index("c")
    left = turned(own, "x", 1)
    right = turned(own, "x", -1)
    far_low = turned(left[:half], "x", 1)
    far_high = turned(right[half:], "x", -1)
    far = jnp.concatenate([far_low, far_high], axis=0)
    whole = jnp.zeros((4, *own.shape), own.dtype)
    for steps, block in ((0, own), (3, left), (1, right), (2, far)):
        whole = lax.dynamic_update_index_in_dim(whole, block, (x + steps) % 4, 0)
    other = turned(whole, "c", 1)
    first = jnp.where(c == 0, whole, other)
    second = jnp.where(c == 0, other, whole)
    return jnp.stack([first, second], axis=1)


def scatter_cb(parts):
    x = lax.axis_index("x")
    c = lax.axis_index("c")
    mine = jnp.where(c == 0, parts[:, 0], parts[:, 1])
    sent = jnp.where(c == 0, parts[:, 1], parts[:, 0])
    pair = (mine.astype(F32) + turned(sent, "c", 1).astype(F32)).astype(BF)
    half = pair.shape[1] // 2
    far = at(pair, (x + 2) % 4)
    from_left = turned(far[:half], "x", 1)
    from_right = turned(far[half:], "x", -1)
    to_right = at(pair, (x + 1) % 4)
    to_left = at(pair, (x + 3) % 4)
    low = (to_right[:half].astype(F32) + from_left.astype(F32)).astype(BF)
    high = (to_left[half:].astype(F32) + from_right.astype(F32)).astype(BF)
    a = turned(jnp.concatenate([low, to_right[half:]], axis=0), "x", 1)
    b = turned(jnp.concatenate([to_left[:half], high], axis=0), "x", -1)
    return at(pair, x).astype(F32) + a.astype(F32) + b.astype(F32)


def valid_taps(values, taps):
    width = taps.shape[0]
    length = values.shape[0] - width + 1
    total = taps[0][None, :] * values[0:length]
    for k in range(1, width):
        total = total + taps[k][None, :] * values[k : k + length]
    return total


def per_device(
    tokens,
    norm_gain,
    up_weight,
    gate_weight,
    up_scale,
    gate_scale,
    up_taps,
    gate_taps,
    down_weight,
    down_scale,
):
    layers = up_weight.shape[0]
    ra = lax.axis_size("z") * lax.axis_size("y")
    cb = lax.axis_index("x") * 2 + lax.axis_index("c")
    rows, hid = up_weight.shape[1:]
    width = rows * ra
    part = rows // 8
    span = tokens.shape[1] // ra
    shards = [
        jnp.concatenate([w[l].astype(BF) for w in (up_weight, gate_weight, down_weight)], axis=1)
        for l in range(layers)
    ]
    weights = [lax.all_gather(s, RA, axis=0, tiled=True) for s in shards]
    own = lax.dynamic_slice_in_dim(tokens, cb * part, part, 0)
    own = own.reshape(part, ra, span).transpose(1, 0, 2)
    own = lax.all_to_all(own, RA, split_axis=0, concat_axis=0, tiled=True)
    every = gather_cb(own)
    state = every.reshape(8, ra, part, span).transpose(3, 1, 0, 2).reshape(span, width)
    edge = up_taps.shape[1] - 1
    for l in range(layers):
        before = shifted(state[span - edge :], RA, 1)
        rows_all = jnp.concatenate([before, state], axis=0)
        rows_f = rows_all.astype(F32)
        inverse = lax.rsqrt(jnp.mean(rows_f * rows_f, axis=1, keepdims=True) + EPS)
        scaled = (rows_f * norm_gain[l][None, :]).astype(BF)
        w = weights[l]
        up_raw = jnp.dot(scaled, w[:, :hid], preferred_element_type=F32)
        gate_raw = jnp.dot(scaled, w[:, hid : 2 * hid], preferred_element_type=F32)
        conv_up = valid_taps(up_raw * inverse * up_scale[l][None, :], up_taps[l])
        conv_gate = valid_taps(gate_raw * inverse * gate_scale[l][None, :], gate_taps[l])
        hidden = (jax.nn.silu(conv_gate) * conv_up).astype(BF)
        down_w = w[:, 2 * hid :]
        if l + 1 < layers:
            down = lax.dot_general(
                hidden, down_w, (((1,), (1,)), ((), ())), preferred_element_type=F32
            ).astype(BF)
            piece = scatter_cb(down.reshape(4, 2, span // 8, width))
            held = lax.dynamic_slice_in_dim(state, cb * (span // 8), span // 8, 0)
            piece = (piece * down_scale[l][None, :] + RESIDUAL * held.astype(F32)).astype(BF)
            state = gather_cb(piece).reshape(span, width)
        else:
            down = lax.dot_general(
                down_w, hidden, (((1,), (1,)), ((), ())), preferred_element_type=F32
            ).astype(BF)
            down = down.reshape(ra, 4, 2, part, span).transpose(1, 2, 0, 3, 4)
            piece = scatter_cb(down)
            held = lax.dynamic_index_in_dim(
                state.reshape(span, ra, 8, part), cb, 2, keepdims=False
            ).transpose(1, 2, 0)
            scale = lax.dynamic_index_in_dim(
                down_scale[l].reshape(ra, 8, part), cb, 1, keepdims=False
            )
            piece = (piece * scale[:, :, None] + RESIDUAL * held.astype(F32)).astype(BF)
    piece = lax.all_to_all(piece, RA, split_axis=0, concat_axis=0, tiled=True)
    piece = piece.transpose(1, 0, 2).reshape(part, ra * span)
    return gather_cb(piece).reshape(rows, ra * span)


def solution(mesh):
    torus = Mesh(mesh.devices.reshape(8, 4, 4, 2), ("z", "y", "x", "c"))
    placed = (
        P(RA, None),
        P(),
        P(None, RA, CB),
        P(None, RA, CB),
        P(None, CB),
        P(None, CB),
        P(None, None, CB),
        P(None, None, CB),
        P(None, RA, CB),
        P(),
    )
    return jax.shard_map(
        per_device, mesh=torus, in_specs=placed, out_specs=P(RA, None), check_vma=False
    )
```

profile of v0, /device:TPU:1, one launch (start us, length us, event | category | flops | bytes accessed | tf_op | source)
XLA Modules:
  0.0 315.6 jit_solution(3003010898439355616)
XLA Ops:
  6.5 1.2 convert.21
  7.7 1.0 convert.22
  8.7 1.0 convert.20
  11.5 23.3 %all_to_all.10 = bf16[32,8,512]{2,1,0:T(8,128)(2,1)S(1)} all-to-all(bf16[32,8,512]{2,1,0:T(8,128)(2,1)S(1)} %bitcast.156), channel_id=1, replica_groups=mesh['z'=8,'y'=4,'x'=4,'c'=2] {'z','y'}, dimensions={0} | all-to-all | bytes 524288 | tf_op jit(solution)/shard_map/all_to_all | solution.py:102
  34.8 1.2 collective-permute-start
  36.0 1.5 collective-permute-start.1
  37.5 4.0 %collective-permute-done = bf16[32,8,512]{2,1,0:T(8,128)(2,1)S(1)} collective-permute-done((bf16[32,8,512]{2,1,0:T(8,128)(2,1)S(1)}, bf16[32,8,512]{2,1,0:T(8,128)(2,1)S(1)}, u32[]{:S(2)}, u32[]{:S(2)}) %collective-permute-start) | collective-permute-done | bytes 262176 | tf_op jit(solution)/shard_map/ppermute | solution.py:17
  41.7 2.7 collective-permute-start.3
  44.5 2.2 collective-permute-done.2
  46.7 4.6 %collective-permute-start.4 = (bf16[4,32,8,512]{3,2,1,0:T(8,128)(2,1)S(1)}, bf16[4,32,8,512]{3,2,1,0:T(8,128)(2,1)S(1)}, u32[]{:S(2)}, u32[]{:S(2)}) collective-permute-start(bf16[4,32,8,512]{3,2,1,0:T(8,128)(2,1)S(1)} %fusion.75), channel_id=1, source_target_pairs={{0,1},{1,0},{2,3},{3,2},{4,5},{5,4},{6,7},{7,6},{8,9},{9,8},{10,11... | collective-permute-start | bytes 3145736 | tf_op jit(solution)/shard_map/ppermute | solution.py:17
  51.5 2.1 collective-permute-done.4
  54.4 1.7 copy.53
  56.3 2.7 collective-permute-start.5
  59.0 1.9 copy.54
  61.2 1.5 fusion.1
  62.8 54.4 %all-gather.5.cloned.1.call-done = bf16[2048,2304]{1,0:T(8,128)(2,1)} async-done(((bf16[64,2304]{1,0:T(8,128)(2,1)}), bf16[2048,2304]{1,0:T(8,128)(2,1)}) %all-gather.5.cloned.1.call-update) | async-done | bytes 9437200 | tf_op jit(solution)/shard_map/all_gather | solution.py:99
  117.2 5.2 %multiply_multiply_fusion.3 = f32[514,768]{1,0:T(8,128)S(1)} fusion(bf16[2048,2304]{1,0:T(8,128)(2,1)} %all-gather.5.cloned.1.call-done, f32[768]{0:T(1024)S(1)} %get-tuple-element.18, f32[514]{0:T(1024)S(1)} %add_rsqrt_fusion.1, f32[2048]{0:T(1024)S(1)} %bitcast.163, bf16[512,2048]{0,1:T(8,128)(2,1)S(1)} %bitcast.144, bf16[2,2048]{0,1:T(8,128)(2,1)S(1)} %copy.55), kind=kOutput, calls=%fused_computation.36 | convolution fusion | flops 1624009728 | bytes 6843400 | tf_op jit(solution)/shard_map/dot_general | solution.py:114
  122.4 3.2 %multiply_multiply_fusion.2 = f32[514,768]{1,0:T(8,128)S(1)} fusion(bf16[2048,2304]{1,0:T(8,128)(2,1)S(1)} %copy-done.14, f32[768]{0:T(1024)S(1)} %get-tuple-element.19, f32[514]{0:T(1024)S(1)} %add_rsqrt_fusion.1, f32[2048]{0:T(1024)S(1)} %bitcast.164, bf16[512,2048]{0,1:T(8,128)(2,1)S(1)} %bitcast.145, bf16[2,2048]{0,1:T(8,128)(2,1)S(1)} %copy.55), kind=kOutput, calls=%fused_computation.35 | convolution fusion | flops 1624009728 | bytes 7362560 | tf_op jit(solution)/shard_map/dot_general | solution.py:113
  125.7 2.7 fusion.20
  128.4 1.2 fusion.87
  129.6 2.0 copy.68
  131.6 1.8 copy.69
  133.4 1.5 select_bitcast_fusion
  134.9 1.9 copy.58
  136.8 3.3 %collective-permute-start.6 = (bf16[4,64,2048]{2,1,0:T(8,128)(2,1)S(1)}, bf16[4,64,2048]{2,1,0:T(8,128)(2,1)}, u32[]{:S(2)}, u32[]{:S(2)}) collective-permute-start(bf16[4,64,2048]{2,1,0:T(8,128)(2,1)S(1)} %copy.58), channel_id=1, source_target_pairs={{0,1},{1,0},{2,3},{3,2},{4,5},{5,4},{6,7},{7,6},{8,9},{9,8},{10,11... | collective-permute-start | bytes 3145736 | tf_op jit(solution)/shard_map/ppermute | solution.py:17
  140.1 2.4 collective-permute-done.6
  142.5 2.7 copy.59
  145.2 3.1 fusion.4
  148.7 1.2 collective-permute-start.7
  150.0 1.5 collective-permute-start.9
  151.5 12.3 %collective-permute-done.7 = bf16[32,2048]{0,1:T(8,128)(2,1)S(1)} collective-permute-done((bf16[32,2048]{0,1:T(8,128)(2,1)S(1)}, bf16[32,2048]{0,1:T(8,128)(2,1)S(1)}, u32[]{:S(2)}, u32[]{:S(2)}) %collective-permute-start.7) | collective-permute-done | bytes 131104 | tf_op jit(solution)/shard_map/ppermute | solution.py:17
  165.7 1.9 collective-permute-start.10
  167.7 11.2 %collective-permute-done.8 = bf16[64,2048]{0,1:T(8,128)(2,1)S(1)} collective-permute-done((bf16[64,2048]{0,1:T(8,128)(2,1)S(1)}, bf16[64,2048]{0,1:T(8,128)(2,1)S(1)}, u32[]{:S(2)}, u32[]{:S(2)}) %collective-permute-start.8) | collective-permute-done | bytes 262176 | tf_op jit(solution)/shard_map/ppermute | solution.py:17
  178.8 1.7 fusion.55
  180.5 2.8 collective-permute-start.12
  183.7 9.4 %collective-permute-done.12 = bf16[64,2048]{0,1:T(8,128)(2,1)S(1)} collective-permute-done((bf16[64,2048]{0,1:T(8,128)(2,1)S(1)}, bf16[64,2048]{0,1:T(8,128)(2,1)S(1)}, u32[]{:S(2)}, u32[]{:S(2)}) %collective-permute-start.12) | collective-permute-done | bytes 262176 | tf_op jit(solution)/shard_map/ppermute | solution.py:17
  194.1 3.5 %collective-permute-start.14 = (bf16[32,2048]{0,1:T(8,128)(2,1)}, bf16[32,2048]{0,1:T(8,128)(2,1)S(1)}, u32[]{:S(2)}, u32[]{:S(2)}) collective-permute-start(bf16[32,2048]{0,1:T(8,128)(2,1)} %slice.372), channel_id=1, source_target_pairs={{0,6},{2,0},{4,2},{6,4},{1,7},{3,1},{5,3},{7,5},{8,14},{10,8},{12,... | collective-permute-start | bytes 393224 | tf_op jit(solution)/shard_map/ppermute | solution.py:17
  198.4 1.3 copy.61
  199.9 6.9 %collective-permute-done.14 = bf16[32,2048]{0,1:T(8,128)(2,1)S(1)} collective-permute-done((bf16[32,2048]{0,1:T(8,128)(2,1)}, bf16[32,2048]{0,1:T(8,128)(2,1)S(1)}, u32[]{:S(2)}, u32[]{:S(2)}) %collective-permute-start.14) | collective-permute-done | bytes 131104 | tf_op jit(solution)/shard_map/ppermute | solution.py:17
  206.9 3.9 %collective-permute-done.13 = bf16[32,2048]{0,1:T(8,128)(2,1)S(1)} collective-permute-done((bf16[32,2048]{0,1:T(8,128)(2,1)}, bf16[32,2048]{0,1:T(8,128)(2,1)S(1)}, u32[]{:S(2)}, u32[]{:S(2)}) %collective-permute-start.13) | collective-permute-done | bytes 131104 | tf_op jit(solution)/shard_map/ppermute | solution.py:17
  211.3 3.4 %collective-permute-start.15 = (bf16[4,64,2048]{2,1,0:T(8,128)(2,1)S(1)}, bf16[4,64,2048]{2,1,0:T(8,128)(2,1)S(1)}, u32[]{:S(2)}, u32[]{:S(2)}) collective-permute-start(bf16[4,64,2048]{2,1,0:T(8,128)(2,1)S(1)} %constant_dynamic-update-slice_fusion.1), channel_id=1, source_target_pairs={{0,1},{1,0},{2,3},{3,2},{4,5},{5,4},{6,7},{7,6},{8,9},{9,8},{10,11... | collective-permute-start | bytes 3145736 | tf_op jit(solution)/shard_map/ppermute | solution.py:17
  214.8 2.3 collective-permute-done.15
  217.4 2.2 collective-permute-start.16
  220.9 4.0 %multiply_multiply_fusion.1 = f32[514,768]{1,0:T(8,128)S(1)} fusion(bf16[2048,2304]{1,0:T(8,128)(2,1)} %all-gather.3.cloned.1.call-done, f32[2048]{0:T(1024)S(1)} %bitcast.161, f32[768]{0:T(1024)S(1)} %get-tuple-element.17, f32[514]{0:T(1024)S(1)} %add_rsqrt_fusion, bf16[512,2048]{1,0:T(8,128)(2,1)S(1)} %bitcast.139, ...), kind=kOutput, calls=%fused_computation.34 | convolution fusion | flops 1624009728 | bytes 6843400 | tf_op jit(solution)/shard_map/dot_general | solution.py:114
  225.5 2.0 multiply_multiply_fusion
  227.5 2.3 fusion.17
  230.0 1.3 copy-done.2
  231.5 1.3 collective-permute-start.17
  232.8 2.4 collective-permute-done.17
  235.2 2.3 fusion.23
  238.2 2.1 collective-permute-start.20
  240.3 3.2 %collective-permute-done.18 = bf16[16,8,512]{2,1,0:T(8,128)(2,1)S(1)} collective-permute-done((bf16[16,8,512]{2,1,0:T(8,128)(2,1)S(1)}, bf16[16,8,512]{2,1,0:T(8,128)(2,1)S(1)}, u32[]{:S(2)}, u32[]{:S(2)}) %collective-permute-start.18) | collective-permute-done | bytes 131104 | tf_op jit(solution)/shard_map/ppermute | solution.py:17
  244.7 2.6 collective-permute-start.21
  247.4 7.5 %copy.66 = bf16[4,2,64,2048]{2,1,0,3:T(2,128)(2,1)} copy(bf16[4,2,64,2048]{3,2,1,0:T(8,128)(2,1)S(1)} %pad_maximum_fusion.3) | data formatting | bytes 4194304 | tf_op jit(solution)/shard_map/stack | solution.py:45
  254.9 9.3 %reshape_reshape.3 = bf16[512,32,8,8]{0,3,2,1:T(8,128)(2,1)S(1)} reshape(bf16[4,2,64,2048]{2,1,0,3:T(2,128)(2,1)} %copy.66) | data formatting | bytes 4194304 | tf_op jit(solution)/shard_map/reshape;reshape | solution.py:134
  264.3 1.2 fusion.72
  265.5 19.9 %all_to_all.11 = bf16[32,8,512]{2,1,0:T(8,128)(2,1)S(1)} all-to-all(bf16[32,8,512]{2,1,0:T(8,128)(2,1)S(1)} %fusion.72), channel_id=1, replica_groups=mesh['z'=8,'y'=4,'x'=4,'c'=2] {'z','y'}, dimensions={0} | all-to-all | bytes 524288 | tf_op jit(solution)/shard_map/all_to_all | solution.py:140
  285.4 2.7 collective-permute-start.23
  288.2 3.6 %collective-permute-done.22 = bf16[8,16384]{1,0:T(8,128)(2,1)S(1)} collective-permute-done((bf16[8,16384]{1,0:T(8,128)(2,1)S(1)}, bf16[8,16384]{1,0:T(8,128)(2,1)S(1)}, u32[]{:S(2)}, u32[]{:S(2)}) %collective-permute-start.22) | collective-permute-done | bytes 262176 | tf_op jit(solution)/shard_map/ppermute | solution.py:17
  292.1 2.7 collective-permute-start.25
  294.9 2.6 collective-permute-done.24
  297.6 6.1 %collective-permute-start.26 = (bf16[4,8,16384]{2,1,0:T(8,128)(2,1)S(1)}, bf16[4,8,16384]{2,1,0:T(8,128)(2,1)S(1)}, u32[]{:S(2)}, u32[]{:S(2)}) collective-permute-start(bf16[4,8,16384]{2,1,0:T(8,128)(2,1)S(1)} %fusion.76), channel_id=1, source_target_pairs={{0,1},{1,0},{2,3},{3,2},{4,5},{5,4},{6,7},{7,6},{8,9},{9,8},{10,11... | collective-permute-start | bytes 3145736 | tf_op jit(solution)/shard_map/ppermute | solution.py:17
  303.8 2.3 collective-permute-done.26
  306.2 1.5 pad_maximum_fusion.4
  (113 shorter events, 14.5 us)
Async XLA Ops:
  6.5 4.9 %copy-start = (bf16[64,16384]{1,0:T(8,128)(2,1)S(1)}, bf16[64,16384]{1,0:T(8,128)(2,1)}, u32[]{:S(2)}) copy-start(bf16[64,16384]{1,0:T(8,128)(2,1)} %param.10) | copy-start | bytes 6291460
  6.5 110.7 %all-gather.5.cloned.1.call-start = ((), (), s32[]{:S(2)}) async-start(), calls=%async_computation.3 | async-start | bytes 9732096 | tf_op jit(solution)/shard_map/all_gather | solution.py:99
  10.6 210.3 %all-gather.3.cloned.1.call-start = ((), (), s32[]{:S(2)}) async-start(), calls=%async_computation.2 | async-start | bytes 9732096 | tf_op jit(solution)/shard_map/all_gather | solution.py:99
  11.4 39.9 %copy-start.11 = (f32[2,768]{1,0:T(2,128)S(1)}, f32[2,768]{1,0:T(2,128)}, u32[]{:S(2)}) copy-start(f32[2,768]{1,0:T(2,128)} %param.15) | copy-start | bytes 18436
  11.5 39.9 %copy-start.7 = (f32[2,3,768]{2,0,1:T(2,128)S(1)}, f32[2,3,768]{2,0,1:T(2,128)}, u32[]{:S(2)}) copy-start(f32[2,3,768]{2,0,1:T(2,128)} %param.16) | copy-start | bytes 55300
  11.5 39.9 %copy-start.8 = (f32[2,3,768]{2,0,1:T(2,128)S(1)}, f32[2,3,768]{2,0,1:T(2,128)}, u32[]{:S(2)}) copy-start(f32[2,3,768]{2,0,1:T(2,128)} %param.17) | copy-start | bytes 55300
  11.5 40.0 %copy-start.9 = (f32[2,2048]{1,0:T(2,128)S(1)}, f32[2,2048]{1,0:T(2,128)}, u32[]{:S(2)}) copy-start(f32[2,2048]{1,0:T(2,128)} %param.11) | copy-start | bytes 49156
  34.8 6.8 %collective-permute-start = (bf16[32,8,512]{2,1,0:T(8,128)(2,1)S(1)}, bf16[32,8,512]{2,1,0:T(8,128)(2,1)S(1)}, u32[]{:S(2)}, u32[]{:S(2)}) collective-permute-start(bf16[32,8,512]{2,1,0:T(8,128)(2,1)S(1)} %all_to_all.10), channel_id=1, source_target_pairs={{0,2},{2,4},{4,6},{6,0},{1,3},{3,5},{5,7},{7,1},{8,10},{10,12},{12... | collective-permute-start | bytes 786440 | tf_op jit(solution)/shard_map/ppermute | solution.py:17
  36.0 5.7 %collective-permute-start.1 = (bf16[32,8,512]{2,1,0:T(8,128)(2,1)S(1)}, bf16[32,8,512]{2,1,0:T(8,128)(2,1)S(1)}, u32[]{:S(2)}, u32[]{:S(2)}) collective-permute-start(bf16[32,8,512]{2,1,0:T(8,128)(2,1)S(1)} %all_to_all.10), channel_id=1, source_target_pairs={{0,6},{2,0},{4,2},{6,4},{1,7},{3,1},{5,3},{7,5},{8,14},{10,8},{12,... | collective-permute-start | bytes 786440 | tf_op jit(solution)/shard_map/ppermute | solution.py:17
  41.6 5.1 %collective-permute-start.2 = (bf16[16,8,512]{2,1,0:T(8,128)(2,1)S(1)}, bf16[16,8,512]{2,1,0:T(8,128)(2,1)S(1)}, u32[]{:S(2)}, u32[]{:S(2)}) collective-permute-start(bf16[16,8,512]{2,1,0:T(8,128)(2,1)S(1)} %slice.354), channel_id=1, source_target_pairs={{0,2},{2,4},{4,6},{6,0},{1,3},{3,5},{5,7},{7,1},{8,10},{10,12},{12... | collective-permute-start | bytes 393224 | tf_op jit(solution)/shard_map/ppermute | solution.py:17
  41.7 5.0 %collective-permute-start.3 = (bf16[16,8,512]{2,1,0:T(8,128)(2,1)S(1)}, bf16[16,8,512]{2,1,0:T(8,128)(2,1)S(1)}, u32[]{:S(2)}, u32[]{:S(2)}) collective-permute-start(bf16[16,8,512]{2,1,0:T(8,128)(2,1)S(1)} %slice.355), channel_id=1, source_target_pairs={{0,6},{2,0},{4,2},{6,4},{1,7},{3,1},{5,3},{7,5},{8,14},{10,8},{12,... | collective-permute-start | bytes 393224 | tf_op jit(solution)/shard_map/ppermute | solution.py:17
  46.7 6.9 %collective-permute-start.4 = (bf16[4,32,8,512]{3,2,1,0:T(8,128)(2,1)S(1)}, bf16[4,32,8,512]{3,2,1,0:T(8,128)(2,1)S(1)}, u32[]{:S(2)}, u32[]{:S(2)}) collective-permute-start(bf16[4,32,8,512]{3,2,1,0:T(8,128)(2,1)S(1)} %fusion.75), channel_id=1, source_target_pairs={{0,1},{1,0},{2,3},{3,2},{4,5},{5,4},{6,7},{7,6},{8,9},{9,8},{10,11... | collective-permute-start | bytes 3145736 | tf_op jit(solution)/shard_map/ppermute | solution.py:17
  53.9 5.0 %copy-start.12 = (f32[2,768]{1,0:T(2,128)S(1)}, f32[2,768]{1,0:T(2,128)}, u32[]{:S(2)}) copy-start(f32[2,768]{1,0:T(2,128)} %param.14) | copy-start | bytes 18436
  54.2 4.8 %copy-start.5 = (bf16[4,2,32,8,512]{4,3,2,1,0:T(8,128)(2,1)}, bf16[4,2,32,8,512]{4,3,2,1,0:T(8,128)(2,1)S(1)}, u32[]{:S(2)}) copy-start(bf16[4,2,32,8,512]{4,3,2,1,0:T(8,128)(2,1)S(1)} %copy.52) | copy-start | bytes 6291460
  56.3 4.6 %collective-permute-start.5 = (bf16[2,2048]{1,0:T(2,128)(2,1)S(1)}, bf16[2,2048]{1,0:T(2,128)(2,1)S(1)}, u32[]{:S(2)}, u32[]{:S(2)}) collective-permute-start(bf16[2,2048]{1,0:T(2,128)(2,1)S(1)} %slice.282), channel_id=1, source_target_pairs={{0,8},{8,16},{16,24},{24,32},{32,40},{40,48},{48,56},{56,64},{64,7... | collective-permute-start | bytes 24584 | tf_op jit(solution)/shard_map/ppermute | solution.py:23
  60.9 61.6 %copy-start.4 = (bf16[512,32,8,8]{0,3,2,1:T(8,128)(2,1)}, bf16[512,32,8,8]{0,3,2,1:T(8,128)(2,1)S(1)}, u32[]{:S(2)}) copy-start(bf16[512,32,8,8]{0,3,2,1:T(8,128)(2,1)S(1)} %copy.54) | copy-start | bytes 6291460
  117.2 5.2 %copy-start.14 = (bf16[2048,2304]{1,0:T(8,128)(2,1)S(1)}, bf16[2048,2304]{1,0:T(8,128)(2,1)}, u32[]{:S(2)}) copy-start(bf16[2048,2304]{1,0:T(8,128)(2,1)} %all-gather.5.cloned.1.call-done) | copy-start | bytes 28311556
  136.8 5.7 %collective-permute-start.6 = (bf16[4,64,2048]{2,1,0:T(8,128)(2,1)S(1)}, bf16[4,64,2048]{2,1,0:T(8,128)(2,1)}, u32[]{:S(2)}, u32[]{:S(2)}) collective-permute-start(bf16[4,64,2048]{2,1,0:T(8,128)(2,1)S(1)} %copy.58), channel_id=1, source_target_pairs={{0,1},{1,0},{2,3},{3,2},{4,5},{5,4},{6,7},{7,6},{8,9},{9,8},{10,11... | collective-permute-start | bytes 3145736 | tf_op jit(solution)/shard_map/ppermute | solution.py:17
  148.3 15.5 %copy-start.3 = (bf16[4,64,2048]{1,2,0:T(8,128)(2,1)}, bf16[4,64,2048]{1,2,0:T(8,128)(2,1)S(1)}, u32[]{:S(2)}) copy-start(bf16[4,64,2048]{1,2,0:T(8,128)(2,1)S(1)} %fusion.4) | copy-start | bytes 3145732
  148.7 15.1 %collective-permute-start.7 = (bf16[32,2048]{0,1:T(8,128)(2,1)S(1)}, bf16[32,2048]{0,1:T(8,128)(2,1)S(1)}, u32[]{:S(2)}, u32[]{:S(2)}) collective-permute-start(bf16[32,2048]{0,1:T(8,128)(2,1)S(1)} %get-tuple-element.27), channel_id=1, source_target_pairs={{0,2},{2,4},{4,6},{6,0},{1,3},{3,5},{5,7},{7,1},{8,10},{10,12},{12... | collective-permute-start | bytes 393224 | tf_op jit(solution)/shard_map/ppermute | solution.py:17
  150.0 13.8 %collective-permute-start.9 = (bf16[32,2048]{0,1:T(8,128)(2,1)S(1)}, bf16[32,2048]{0,1:T(8,128)(2,1)S(1)}, u32[]{:S(2)}, u32[]{:S(2)}) collective-permute-start(bf16[32,2048]{0,1:T(8,128)(2,1)S(1)} %get-tuple-element.29), channel_id=1, source_target_pairs={{0,6},{2,0},{4,2},{6,4},{1,7},{3,1},{5,3},{7,5},{8,14},{10,8},{12,... | collective-permute-start | bytes 393224 | tf_op jit(solution)/shard_map/ppermute | solution.py:17
  164.2 3.4 %copy-start.10 = (f32[2,2048]{1,0:T(2,128)S(1)}, f32[2,2048]{1,0:T(2,128)}, u32[]{:S(2)}) copy-start(f32[2,2048]{1,0:T(2,128)} %param.19) | copy-start | bytes 49156
  164.5 14.3 %collective-permute-start.8 = (bf16[64,2048]{0,1:T(8,128)(2,1)S(1)}, bf16[64,2048]{0,1:T(8,128)(2,1)S(1)}, u32[]{:S(2)}, u32[]{:S(2)}) collective-permute-start(bf16[64,2048]{0,1:T(8,128)(2,1)S(1)} %pad_maximum_fusion.7), channel_id=1, source_target_pairs={{0,2},{2,4},{4,6},{6,0},{1,3},{3,5},{5,7},{7,1},{8,10},{10,12},{12... | collective-permute-start | bytes 786440 | tf_op jit(solution)/shard_map/ppermute | solution.py:17
  165.7 13.1 %collective-permute-start.10 = (bf16[64,2048]{0,1:T(8,128)(2,1)S(1)}, bf16[64,2048]{0,1:T(8,128)(2,1)S(1)}, u32[]{:S(2)}, u32[]{:S(2)}) collective-permute-start(bf16[64,2048]{0,1:T(8,128)(2,1)S(1)} %pad_maximum_fusion.8), channel_id=1, source_target_pairs={{0,6},{2,0},{4,2},{6,4},{1,7},{3,1},{5,3},{7,5},{8,14},{10,8},{12,... | collective-permute-start | bytes 786440 | tf_op jit(solution)/shard_map/ppermute | solution.py:17
  180.5 12.5 %collective-permute-start.12 = (bf16[64,2048]{0,1:T(8,128)(2,1)S(1)}, bf16[64,2048]{0,1:T(8,128)(2,1)S(1)}, u32[]{:S(2)}, u32[]{:S(2)}) collective-permute-start(bf16[64,2048]{0,1:T(8,128)(2,1)S(1)} %fusion.55), channel_id=1, source_target_pairs={{0,6},{2,0},{4,2},{6,4},{1,7},{3,1},{5,3},{7,5},{8,14},{10,8},{12,... | collective-permute-start | bytes 786440 | tf_op jit(solution)/shard_map/ppermute | solution.py:17
  183.4 14.2 %collective-permute-start.11 = (bf16[64,2048]{0,1:T(8,128)(2,1)S(1)}, bf16[64,2048]{0,1:T(8,128)(2,1)S(1)}, u32[]{:S(2)}, u32[]{:S(2)}) collective-permute-start(bf16[64,2048]{0,1:T(8,128)(2,1)S(1)} %fusion.55), channel_id=1, source_target_pairs={{0,2},{2,4},{4,6},{6,0},{1,3},{3,5},{5,7},{7,1},{8,10},{10,12},{12... | collective-permute-start | bytes 786440 | tf_op jit(solution)/shard_map/ppermute | solution.py:17
  194.1 12.8 %collective-permute-start.14 = (bf16[32,2048]{0,1:T(8,128)(2,1)}, bf16[32,2048]{0,1:T(8,128)(2,1)S(1)}, u32[]{:S(2)}, u32[]{:S(2)}) collective-permute-start(bf16[32,2048]{0,1:T(8,128)(2,1)} %slice.372), channel_id=1, source_target_pairs={{0,6},{2,0},{4,2},{6,4},{1,7},{3,1},{5,3},{7,5},{8,14},{10,8},{12,... | collective-permute-start | bytes 393224 | tf_op jit(solution)/shard_map/ppermute | solution.py:17
  197.6 0.8 copy-start.6
  198.4 12.4 %collective-permute-start.13 = (bf16[32,2048]{0,1:T(8,128)(2,1)}, bf16[32,2048]{0,1:T(8,128)(2,1)S(1)}, u32[]{:S(2)}, u32[]{:S(2)}) collective-permute-start(bf16[32,2048]{0,1:T(8,128)(2,1)} %bitcast.157), channel_id=1, source_target_pairs={{0,2},{2,4},{4,6},{6,0},{1,3},{3,5},{5,7},{7,1},{8,10},{10,12},{12... | collective-permute-start | bytes 393224 | tf_op jit(solution)/shard_map/ppermute | solution.py:17
  211.3 5.7 %collective-permute-start.15 = (bf16[4,64,2048]{2,1,0:T(8,128)(2,1)S(1)}, bf16[4,64,2048]{2,1,0:T(8,128)(2,1)S(1)}, u32[]{:S(2)}, u32[]{:S(2)}) collective-permute-start(bf16[4,64,2048]{2,1,0:T(8,128)(2,1)S(1)} %constant_dynamic-update-slice_fusion.1), channel_id=1, source_target_pairs={{0,1},{1,0},{2,3},{3,2},{4,5},{5,4},{6,7},{7,6},{8,9},{9,8},{10,11... | collective-permute-start | bytes 3145736 | tf_op jit(solution)/shard_map/ppermute | solution.py:17
  217.4 2.6 collective-permute-start.16
  220.9 4.6 %copy-start.13 = (bf16[2048,2304]{1,0:T(8,128)(2,1)S(1)}, bf16[2048,2304]{1,0:T(8,128)(2,1)}, u32[]{:S(2)}) copy-start(bf16[2048,2304]{1,0:T(8,128)(2,1)} %all-gather.3.cloned.1.call-done) | copy-start | bytes 28311556
  230.0 1.3 copy-start.2
  231.5 3.7 %collective-permute-start.17 = (bf16[4,32,8,512]{3,2,1,0:T(8,128)(2,1)S(1)}, bf16[4,32,8,512]{3,2,1,0:T(8,128)(2,1)}, u32[]{:S(2)}, u32[]{:S(2)}) collective-permute-start(bf16[4,32,8,512]{3,2,1,0:T(8,128)(2,1)S(1)} %select_bitcast_fusion.3), channel_id=1, source_target_pairs={{0,1},{1,0},{2,3},{3,2},{4,5},{5,4},{6,7},{7,6},{8,9},{9,8},{10,11... | collective-permute-start | bytes 3145736 | tf_op jit(solution)/shard_map/ppermute | solution.py:17
  237.6 6.0 %collective-permute-start.18 = (bf16[16,8,512]{2,1,0:T(8,128)(2,1)S(1)}, bf16[16,8,512]{2,1,0:T(8,128)(2,1)S(1)}, u32[]{:S(2)}, u32[]{:S(2)}) collective-permute-start(bf16[16,8,512]{2,1,0:T(8,128)(2,1)S(1)} %get-tuple-element.37), channel_id=1, source_target_pairs={{0,2},{2,4},{4,6},{6,0},{1,3},{3,5},{5,7},{7,1},{8,10},{10,12},{12... | collective-permute-start | bytes 393224 | tf_op jit(solution)/shard_map/ppermute | solution.py:17
  238.2 5.4 %collective-permute-start.20 = (bf16[16,8,512]{2,1,0:T(8,128)(2,1)S(1)}, bf16[16,8,512]{2,1,0:T(8,128)(2,1)S(1)}, u32[]{:S(2)}, u32[]{:S(2)}) collective-permute-start(bf16[16,8,512]{2,1,0:T(8,128)(2,1)S(1)} %get-tuple-element.39), channel_id=1, source_target_pairs={{0,6},{2,0},{4,2},{6,4},{1,7},{3,1},{5,3},{7,5},{8,14},{10,8},{12,... | collective-permute-start | bytes 393224 | tf_op jit(solution)/shard_map/ppermute | solution.py:17
  243.6 20.6 %collective-permute-start.19 = (bf16[32,8,512]{2,1,0:T(8,128)(2,1)S(1)}, bf16[32,8,512]{2,1,0:T(8,128)(2,1)}, u32[]{:S(2)}, u32[]{:S(2)}) collective-permute-start(bf16[32,8,512]{2,1,0:T(8,128)(2,1)S(1)} %pad_maximum_fusion.11), channel_id=1, source_target_pairs={{0,2},{2,4},{4,6},{6,0},{1,3},{3,5},{5,7},{7,1},{8,10},{10,12},{12... | collective-permute-start | bytes 786440 | tf_op jit(solution)/shard_map/ppermute | solution.py:17
  244.7 19.6 %collective-permute-start.21 = (bf16[32,8,512]{2,1,0:T(8,128)(2,1)}, bf16[32,8,512]{2,1,0:T(8,128)(2,1)}, u32[]{:S(2)}, u32[]{:S(2)}) collective-permute-start(bf16[32,8,512]{2,1,0:T(8,128)(2,1)} %pad_maximum_fusion.12), channel_id=1, source_target_pairs={{0,6},{2,0},{4,2},{6,4},{1,7},{3,1},{5,3},{7,5},{8,14},{10,8},{12,... | collective-permute-start | bytes 786440 | tf_op jit(solution)/shard_map/ppermute | solution.py:17
  285.4 6.4 %collective-permute-start.22 = (bf16[8,16384]{1,0:T(8,128)(2,1)S(1)}, bf16[8,16384]{1,0:T(8,128)(2,1)S(1)}, u32[]{:S(2)}, u32[]{:S(2)}) collective-permute-start(bf16[8,16384]{1,0:T(8,128)(2,1)S(1)} %bitcast.153), channel_id=1, source_target_pairs={{0,2},{2,4},{4,6},{6,0},{1,3},{3,5},{5,7},{7,1},{8,10},{10,12},{12... | collective-permute-start | bytes 786440 | tf_op jit(solution)/shard_map/ppermute | solution.py:17
  285.4 6.6 %collective-permute-start.23 = (bf16[8,16384]{1,0:T(8,128)(2,1)S(1)}, bf16[8,16384]{1,0:T(8,128)(2,1)S(1)}, u32[]{:S(2)}, u32[]{:S(2)}) collective-permute-start(bf16[8,16384]{1,0:T(8,128)(2,1)S(1)} %bitcast.154), channel_id=1, source_target_pairs={{0,6},{2,0},{4,2},{6,4},{1,7},{3,1},{5,3},{7,5},{8,14},{10,8},{12,... | collective-permute-start | bytes 786440 | tf_op jit(solution)/shard_map/ppermute | solution.py:17
  291.9 5.6 %collective-permute-start.24 = (bf16[4,16384]{1,0:T(4,128)(2,1)S(1)}, bf16[4,16384]{1,0:T(4,128)(2,1)S(1)}, u32[]{:S(2)}, u32[]{:S(2)}) collective-permute-start(bf16[4,16384]{1,0:T(4,128)(2,1)S(1)} %slice.384), channel_id=1, source_target_pairs={{0,2},{2,4},{4,6},{6,0},{1,3},{3,5},{5,7},{7,1},{8,10},{10,12},{12... | collective-permute-start | bytes 393224 | tf_op jit(solution)/shard_map/ppermute | solution.py:17
  292.1 5.4 %collective-permute-start.25 = (bf16[4,16384]{1,0:T(4,128)(2,1)S(1)}, bf16[4,16384]{1,0:T(4,128)(2,1)S(1)}, u32[]{:S(2)}, u32[]{:S(2)}) collective-permute-start(bf16[4,16384]{1,0:T(4,128)(2,1)S(1)} %slice.385), channel_id=1, source_target_pairs={{0,6},{2,0},{4,2},{6,4},{1,7},{3,1},{5,3},{7,5},{8,14},{10,8},{12,... | collective-permute-start | bytes 393224 | tf_op jit(solution)/shard_map/ppermute | solution.py:17
  297.6 8.4 %collective-permute-start.26 = (bf16[4,8,16384]{2,1,0:T(8,128)(2,1)S(1)}, bf16[4,8,16384]{2,1,0:T(8,128)(2,1)S(1)}, u32[]{:S(2)}, u32[]{:S(2)}) collective-permute-start(bf16[4,8,16384]{2,1,0:T(8,128)(2,1)S(1)} %fusion.76), channel_id=1, source_target_pairs={{0,1},{1,0},{2,3},{3,2},{4,5},{5,4},{6,7},{7,6},{8,9},{9,8},{10,11... | collective-permute-start | bytes 3145736 | tf_op jit(solution)/shard_map/ppermute | solution.py:17
  306.2 2.4 copy-start.1
Sparse Core Ops, SparseCore 0:
  10.7 106.4 all-gather.4
  119.8 100.2 all-gather.2
where the time goes:
time: 321 us; the launch traced here: 316 us
  waiting for transfers between devices  126 us (39%)
  starting transfers between devices  52.2 us (16%)
  blocking collectives  43.2 us (13%)
  local copies, waits for them, and re-layouts  39.1 us (12%)
  other arithmetic  21.6 us (7%)
  matrix products  19.4 us (6%)
  between operations  14.3 us (4%)
    ppermute x25, waiting for transfers between devices, turned(): lax.ppermute(value, axis, [(s, (s + steps) % count) for s in range(count)])  71 us
    all_gather x2, waiting for transfers between devices, per_device(): weights = [lax.all_gather(s, RA, axis=0, tiled=True) for s in shards]  54.4 us
    ppermute x25, starting transfers between devices, turned(): lax.ppermute(value, axis, [(s, (s + steps) % count) for s in range(count)])  47.3 us
    all_to_all x1, blocking collectives, per_device(): own = lax.all_to_all(own, RA, split_axis=0, concat_axis=0, tiled=True)  23.3 us
    all_to_all x1, blocking collectives, per_device(): piece = lax.all_to_all(piece, RA, split_axis=0, concat_axis=0, tiled=True)  19.9 us
    another operation x1, local copies, waits for them, and re-layouts, per_device(): state.reshape(span, ra, 8, part)  9.35 us
    dot_general x2, matrix products, per_device(): gate_raw = jnp.dot(scaled, w[:, hid:2 * hid], preferred_element_type=F32)  9.18 us
    another operation x2, local copies, waits for them, and re-layouts, gather_cb(): return jnp.stack([first, second], axis=1)  7.73 us
  transfers between devices with their start and end apart: 29, of which 17 were waited for; matrix products, arithmetic and copies ran while one was open for 19% of the time, Pallas kernels for 0%

commit v1 on v0

--- a/solution.py
+++ b/solution.py
@@ -96,7 +96,10 @@
         jnp.concatenate([w[l].astype(BF) for w in (up_weight, gate_weight, down_weight)], axis=1)
         for l in range(layers)
     ]
-    weights = [lax.all_gather(s, RA, axis=0, tiled=True) for s in shards]
+    weights = [
+        jnp.concatenate(lax.all_to_all(jnp.stack([s] * lax.axis_size(RA)), RA, 0, 0), axis=0)
+        for s in shards
+    ]
     own = lax.dynamic_slice_in_dim(tokens, cb * part, part, 0)
     own = own.reshape(part, ra, span).transpose(1, 0, 2)
     own = lax.all_to_all(own, RA, split_axis=0, concat_axis=0, tiled=True)

time: 321 us -> 678 us (2.11)
  waiting for transfers between devices: 126 us -> 367 us
  blocking collectives: 43.2 us -> 127 us
  starting transfers between devices: 52.2 us -> 80.5 us
  between operations: 14.3 us -> 0.9 us
  local copies, waits for them, and re-layouts: 39.1 us -> 50 us
  matrix products: 19.4 us -> 26.5 us
    all_to_all x0 -> x3, waiting for transfers between devices: none -> 294 us  [the longest x2 284 us: per_device(): lax.all_to_all(jnp.stack([s] * lax.axis_size(RA)), RA, 0, 0)]
    all_to_all x1, blocking collectives: 19.9 us -> 127 us  [per_device(): piece = lax.all_to_all(piece, RA, split_axis=0, concat_axis=0, tiled=True)]
    all_gather x2 -> x0, waiting for transfers between devices: 54.4 us -> none  [per_device(): weights = [lax.all_gather(s, RA, axis=0, tiled=True) for s in shards]]
    all_to_all x0 -> x3, starting transfers between devices: none -> 23.5 us  [the longest x1 12 us: per_device(): own = lax.all_to_all(own, RA, split_axis=0, concat_axis=0, tiled=True)]
    all_to_all x1 -> x0, blocking collectives: 23.3 us -> none  [per_device(): own = lax.all_to_all(own, RA, split_axis=0, concat_axis=0, tiled=True)]
    another operation x0 -> x2, local copies, waits for them, and re-layouts: none -> 9.39 us  [per_device(): jnp.stack([s] * lax.axis_size(RA))]
  transfers between devices with their start and end apart: 29 -> 30, of which waited for: 17 -> 19; matrix products, arithmetic and copies ran while one was open for 19% -> 9% of each run, Pallas kernels for 0% -> 0%
where the time goes in v1:
time: 678 us; the launch traced here: 671 us
  waiting for transfers between devices  367 us (54%)
  blocking collectives  127 us (19%)
  starting transfers between devices  80.5 us (12%)
  local copies, waits for them, and re-layouts  50 us (7%)
  matrix products  26.5 us (4%)
  other arithmetic  18.9 us (3%)
    all_to_all x2, waiting for transfers between devices, per_device(): lax.all_to_all(jnp.stack([s] * lax.axis_size(RA)), RA, 0, 0)  284 us
    all_to_all x1, blocking collectives, per_device(): piece = lax.all_to_all(piece, RA, split_axis=0, concat_axis=0, tiled=True)  127 us
    ppermute x25, waiting for transfers between devices, turned(): lax.ppermute(value, axis, [(s, (s + steps) % count) for s in range(count)])  73 us
    ppermute x25, starting transfers between devices, turned(): lax.ppermute(value, axis, [(s, (s + steps) % count) for s in range(count)])  50.9 us
  transfers between devices with their start and end apart: 30, of which 19 were waited for; matrix products, arithmetic and copies ran while one was open for 9% of the time, Pallas kernels for 0%

profile of v1, /device:TPU:1, one launch (start us, length us, event | category | flops | bytes accessed | tf_op | source)
XLA Modules:
  0.0 670.6 jit_solution(9980337736769563616)
XLA Ops:
  0.0 1.6 copy-done
  2.3 12.0 %all-to-all-start.1 = ((bf16[32,8,512]{2,1,0:T(8,128)(2,1)}), bf16[32,8,512]{2,1,0:T(8,128)(2,1)S(1)}, u32[]{:S(2)}, u32[]{:S(2)}) async-start(bf16[32,8,512]{2,1,0:T(8,128)(2,1)} %bitcast.5), calls=%async_computation.1 | async-start | bytes 524288 | tf_op jit(solution)/shard_map/all_to_all | solution.py:105
  16.5 9.1 %all-to-all-done.1 = bf16[32,8,512]{2,1,0:T(8,128)(2,1)S(1)} async-done(((bf16[32,8,512]{2,1,0:T(8,128)(2,1)}), bf16[32,8,512]{2,1,0:T(8,128)(2,1)S(1)}, u32[]{:S(2)}, u32[]{:S(2)}) %all-to-all-start.1) | async-done | bytes 262176 | tf_op jit(solution)/shard_map/all_to_all | solution.py:105
  25.7 4.7 stack.26
  30.3 5.0 all-to-all-start.2
  35.3 213.2 %all-to-all-done.2 = bf16[32,64,2304]{2,1,0:T(8,128)(2,1)} async-done(((bf16[32,64,2304]{2,1,0:T(8,128)(2,1)}), bf16[32,64,2304]{2,1,0:T(8,128)(2,1)}, u32[]{:S(2)}, u32[]{:S(2)}) %all-to-all-start.2) | async-done | bytes 9437216 | tf_op jit(solution)/shard_map/all_to_all | solution.py:100
  248.6 4.7 stack.22
  253.3 6.5 all-to-all-start
  261.1 1.5 collective-permute-start.1
  262.7 4.6 collective-permute-done
  267.4 2.7 collective-permute-start.3
  270.2 2.6 collective-permute-done.2
  272.8 3.4 collective-permute-start.4
  276.4 2.1 collective-permute-done.4
  279.3 1.7 copy.53
  281.2 3.2 collective-permute-start.5
  284.5 1.9 copy.54
  286.7 1.5 fusion.1
  288.3 5.1 multiply_multiply_fusion.3
  293.3 5.1 multiply_multiply_fusion.2
  298.4 4.6 fusion.20
  304.2 2.0 copy.68
  306.2 1.8 copy.69
  308.0 1.5 select_bitcast_fusion
  309.5 1.9 copy.58
  311.4 2.5 collective-permute-start.6
  314.0 2.4 collective-permute-done.6
  316.4 2.7 copy.59
  319.1 3.0 fusion.4
  323.4 2.4 collective-permute-start.9
  325.8 12.4 %collective-permute-done.7 = bf16[32,2048]{0,1:T(8,128)(2,1)S(1)} collective-permute-done((bf16[32,2048]{0,1:T(8,128)(2,1)S(1)}, bf16[32,2048]{0,1:T(8,128)(2,1)S(1)}, u32[]{:S(2)}, u32[]{:S(2)}) %collective-permute-start.7) | collective-permute-done | bytes 131104 | tf_op jit(solution)/shard_map/ppermute | solution.py:17
  340.0 2.0 collective-permute-start.10
  342.0 11.5 %collective-permute-done.8 = bf16[64,2048]{0,1:T(8,128)(2,1)S(1)} collective-permute-done((bf16[64,2048]{0,1:T(8,128)(2,1)S(1)}, bf16[64,2048]{0,1:T(8,128)(2,1)S(1)}, u32[]{:S(2)}, u32[]{:S(2)}) %collective-permute-start.8) | collective-permute-done | bytes 262176 | tf_op jit(solution)/shard_map/ppermute | solution.py:17
  353.5 1.7 fusion.55
  355.2 2.8 collective-permute-start.12
  358.4 9.7 %collective-permute-done.12 = bf16[64,2048]{0,1:T(8,128)(2,1)S(1)} collective-permute-done((bf16[64,2048]{0,1:T(8,128)(2,1)S(1)}, bf16[64,2048]{0,1:T(8,128)(2,1)S(1)}, u32[]{:S(2)}, u32[]{:S(2)}) %collective-permute-start.12) | collective-permute-done | bytes 262176 | tf_op jit(solution)/shard_map/ppermute | solution.py:17
  369.1 3.5 collective-permute-start.14
  375.0 7.3 %collective-permute-done.14 = bf16[32,2048]{0,1:T(8,128)(2,1)S(1)} collective-permute-done((bf16[32,2048]{0,1:T(8,128)(2,1)}, bf16[32,2048]{0,1:T(8,128)(2,1)S(1)}, u32[]{:S(2)}, u32[]{:S(2)}) %collective-permute-start.14) | collective-permute-done | bytes 131104 | tf_op jit(solution)/shard_map/ppermute | solution.py:17
  382.2 3.9 collective-permute-done.13
  386.7 3.1 collective-permute-start.15
  389.8 2.3 collective-permute-done.15
  392.5 3.0 collective-permute-start.16
  396.6 71.2 %all-to-all-done = bf16[32,64,2304]{2,1,0:T(8,128)(2,1)} async-done(((bf16[32,64,2304]{2,1,0:T(8,128)(2,1)}), bf16[32,64,2304]{2,1,0:T(8,128)(2,1)}, u32[]{:S(2)}, u32[]{:S(2)}) %all-to-all-start) | async-done | bytes 9437216 | tf_op jit(solution)/shard_map/all_to_all | solution.py:100
  467.9 3.8 multiply_multiply_fusion.1
  471.7 3.8 multiply_multiply_fusion
  475.5 4.2 fusion.17
  479.9 1.3 copy-done.2
  481.3 6.5 collective-permute-start.17
  487.8 2.4 collective-permute-done.17
  490.3 2.3 fusion.23
  492.6 1.3 collective-permute-start.18
  493.9 1.5 collective-permute-start.20
  495.4 3.2 collective-permute-done.18
  500.4 1.9 collective-permute-start.21
  502.5 7.5 %copy.66 = bf16[4,2,64,2048]{2,1,0,3:T(2,128)(2,1)} copy(bf16[4,2,64,2048]{3,2,1,0:T(8,128)(2,1)S(1)} %pad_maximum_fusion.3) | data formatting | bytes 4194304 | tf_op jit(solution)/shard_map/stack | solution.py:45
  509.9 9.3 %reshape_reshape.3 = bf16[512,32,8,8]{0,3,2,1:T(8,128)(2,1)S(1)} reshape(bf16[4,2,64,2048]{2,1,0,3:T(2,128)(2,1)} %copy.66) | data formatting | bytes 4194304 | tf_op jit(solution)/shard_map/reshape;reshape | solution.py:137
  520.5 126.8 %all_to_all.20 = bf16[32,8,512]{2,1,0:T(8,128)(2,1)S(1)} all-to-all(bf16[32,8,512]{2,1,0:T(8,128)(2,1)S(1)} %fusion.72), channel_id=1, replica_groups=mesh['z'=8,'y'=4,'x'=4,'c'=2] {'z','y'}, dimensions={0} | all-to-all | bytes 524288 | tf_op jit(solution)/shard_map/all_to_all | solution.py:143
  647.3 2.7 collective-permute-start.23
  650.1 3.6 collective-permute-done.22
  654.0 2.7 collective-permute-start.25
  656.8 2.6 collective-permute-done.24
  659.5 6.1 collective-permute-start.26
  665.7 2.3 collective-permute-done.26
  668.1 1.5 pad_maximum_fusion.4
  (112 shorter events, 20.8 us)
Async XLA Ops:
  0.0 1.6 copy-start
  0.0 16.4 %copy-start.7 = (f32[2,64,768]{2,1,0:T(8,128)S(1)}, f32[2,64,768]{2,1,0:T(8,128)}, u32[]{:S(2)}) copy-start(f32[2,64,768]{2,1,0:T(8,128)} %param.12) | copy-start | bytes 1179652
  2.3 23.3 %all-to-all-start.1 = ((bf16[32,8,512]{2,1,0:T(8,128)(2,1)}), bf16[32,8,512]{2,1,0:T(8,128)(2,1)S(1)}, u32[]{:S(2)}, u32[]{:S(2)}) async-start(bf16[32,8,512]{2,1,0:T(8,128)(2,1)} %bitcast.5), calls=%async_computation.1 | async-start | bytes 524288 | tf_op jit(solution)/shard_map/all_to_all | solution.py:105
  30.3 218.3 %all-to-all-start.2 = ((bf16[32,64,2304]{2,1,0:T(8,128)(2,1)}), bf16[32,64,2304]{2,1,0:T(8,128)(2,1)}, u32[]{:S(2)}, u32[]{:S(2)}) async-start(bf16[32,64,2304]{2,1,0:T(8,128)(2,1)} %stack.26), calls=%async_computation.2 | async-start | bytes 18874368 | tf_op jit(solution)/shard_map/all_to_all | solution.py:100
  253.3 214.6 %all-to-all-start = ((bf16[32,64,2304]{2,1,0:T(8,128)(2,1)}), bf16[32,64,2304]{2,1,0:T(8,128)(2,1)}, u32[]{:S(2)}, u32[]{:S(2)}) async-start(bf16[32,64,2304]{2,1,0:T(8,128)(2,1)} %stack.22), calls=%async_computation | async-start | bytes 18874368 | tf_op jit(solution)/shard_map/all_to_all | solution.py:100
  259.8 16.4 %copy-start.12 = (f32[2,768]{1,0:T(2,128)S(1)}, f32[2,768]{1,0:T(2,128)}, u32[]{:S(2)}) copy-start(f32[2,768]{1,0:T(2,128)} %param.15) | copy-start | bytes 18436
  259.8 16.5 %copy-start.8 = (f32[2,3,768]{2,0,1:T(2,128)S(1)}, f32[2,3,768]{2,0,1:T(2,128)}, u32[]{:S(2)}) copy-start(f32[2,3,768]{2,0,1:T(2,128)} %param.16) | copy-start | bytes 55300
  259.8 16.5 %copy-start.9 = (f32[2,3,768]{2,0,1:T(2,128)S(1)}, f32[2,3,768]{2,0,1:T(2,128)}, u32[]{:S(2)}) copy-start(f32[2,3,768]{2,0,1:T(2,128)} %param.17) | copy-start | bytes 55300
  259.8 16.6 %copy-start.10 = (f32[2,2048]{1,0:T(2,128)S(1)}, f32[2,2048]{1,0:T(2,128)}, u32[]{:S(2)}) copy-start(f32[2,2048]{1,0:T(2,128)} %param.11) | copy-start | bytes 49156
  259.8 7.4 %collective-permute-start = (bf16[32,8,512]{2,1,0:T(8,128)(2,1)S(1)}, bf16[32,8,512]{2,1,0:T(8,128)(2,1)S(1)}, u32[]{:S(2)}, u32[]{:S(2)}) collective-permute-start(bf16[32,8,512]{2,1,0:T(8,128)(2,1)S(1)} %all-to-all-done.1), channel_id=1, source_target_pairs={{0,2},{2,4},{4,6},{6,0},{1,3},{3,5},{5,7},{7,1},{8,10},{10,12},{12... | collective-permute-start | bytes 786440 | tf_op jit(solution)/shard_map/ppermute | solution.py:17
  261.1 6.2 collective-permute-start.1
  267.3 5.5 collective-permute-start.2
  267.4 5.4 collective-permute-start.3
  272.8 5.7 collective-permute-start.4
  278.8 5.6 copy-start.13
  279.1 5.4 copy-start.5
  281.2 5.2 collective-permute-start.5
  286.4 7.0 %copy-start.4 = (bf16[512,32,8,8]{0,3,2,1:T(8,128)(2,1)}, bf16[512,32,8,8]{0,3,2,1:T(8,128)(2,1)S(1)}, u32[]{:S(2)}) copy-start(bf16[512,32,8,8]{0,3,2,1:T(8,128)(2,1)S(1)} %copy.54) | copy-start | bytes 6291460
  311.4 5.0 collective-permute-start.6
  322.1 16.1 %copy-start.3 = (bf16[4,64,2048]{1,2,0:T(8,128)(2,1)}, bf16[4,64,2048]{1,2,0:T(8,128)(2,1)S(1)}, u32[]{:S(2)}) copy-start(bf16[4,64,2048]{1,2,0:T(8,128)(2,1)S(1)} %fusion.4) | copy-start | bytes 3145732
  322.6 15.6 %collective-permute-start.7 = (bf16[32,2048]{0,1:T(8,128)(2,1)S(1)}, bf16[32,2048]{0,1:T(8,128)(2,1)S(1)}, u32[]{:S(2)}, u32[]{:S(2)}) collective-permute-start(bf16[32,2048]{0,1:T(8,128)(2,1)S(1)} %get-tuple-element.27), channel_id=1, source_target_pairs={{0,2},{2,4},{4,6},{6,0},{1,3},{3,5},{5,7},{7,1},{8,10},{10,12},{12... | collective-permute-start | bytes 393224 | tf_op jit(solution)/shard_map/ppermute | solution.py:17
  323.4 14.8 %collective-permute-start.9 = (bf16[32,2048]{0,1:T(8,128)(2,1)S(1)}, bf16[32,2048]{0,1:T(8,128)(2,1)S(1)}, u32[]{:S(2)}, u32[]{:S(2)}) collective-permute-start(bf16[32,2048]{0,1:T(8,128)(2,1)S(1)} %get-tuple-element.29), channel_id=1, source_target_pairs={{0,6},{2,0},{4,2},{6,4},{1,7},{3,1},{5,3},{7,5},{8,14},{10,8},{12,... | collective-permute-start | bytes 393224 | tf_op jit(solution)/shard_map/ppermute | solution.py:17
  338.6 3.4 copy-start.11
  338.9 14.7 %collective-permute-start.8 = (bf16[64,2048]{0,1:T(8,128)(2,1)S(1)}, bf16[64,2048]{0,1:T(8,128)(2,1)S(1)}, u32[]{:S(2)}, u32[]{:S(2)}) collective-permute-start(bf16[64,2048]{0,1:T(8,128)(2,1)S(1)} %pad_maximum_fusion.7), channel_id=1, source_target_pairs={{0,2},{2,4},{4,6},{6,0},{1,3},{3,5},{5,7},{7,1},{8,10},{10,12},{12... | collective-permute-start | bytes 786440 | tf_op jit(solution)/shard_map/ppermute | solution.py:17
  340.0 13.6 %collective-permute-start.10 = (bf16[64,2048]{0,1:T(8,128)(2,1)S(1)}, bf16[64,2048]{0,1:T(8,128)(2,1)S(1)}, u32[]{:S(2)}, u32[]{:S(2)}) collective-permute-start(bf16[64,2048]{0,1:T(8,128)(2,1)S(1)} %pad_maximum_fusion.8), channel_id=1, source_target_pairs={{0,6},{2,0},{4,2},{6,4},{1,7},{3,1},{5,3},{7,5},{8,14},{10,8},{12,... | collective-permute-start | bytes 786440 | tf_op jit(solution)/shard_map/ppermute | solution.py:17
  355.2 12.9 %collective-permute-start.12 = (bf16[64,2048]{0,1:T(8,128)(2,1)S(1)}, bf16[64,2048]{0,1:T(8,128)(2,1)S(1)}, u32[]{:S(2)}, u32[]{:S(2)}) collective-permute-start(bf16[64,2048]{0,1:T(8,128)(2,1)S(1)} %fusion.55), channel_id=1, source_target_pairs={{0,6},{2,0},{4,2},{6,4},{1,7},{3,1},{5,3},{7,5},{8,14},{10,8},{12,... | collective-permute-start | bytes 786440 | tf_op jit(solution)/shard_map/ppermute | solution.py:17
  358.1 14.6 %collective-permute-start.11 = (bf16[64,2048]{0,1:T(8,128)(2,1)S(1)}, bf16[64,2048]{0,1:T(8,128)(2,1)S(1)}, u32[]{:S(2)}, u32[]{:S(2)}) collective-permute-start(bf16[64,2048]{0,1:T(8,128)(2,1)S(1)} %fusion.55), channel_id=1, source_target_pairs={{0,2},{2,4},{4,6},{6,0},{1,3},{3,5},{5,7},{7,1},{8,10},{10,12},{12... | collective-permute-start | bytes 786440 | tf_op jit(solution)/shard_map/ppermute | solution.py:17
  369.1 13.1 %collective-permute-start.14 = (bf16[32,2048]{0,1:T(8,128)(2,1)}, bf16[32,2048]{0,1:T(8,128)(2,1)S(1)}, u32[]{:S(2)}, u32[]{:S(2)}) collective-permute-start(bf16[32,2048]{0,1:T(8,128)(2,1)} %slice.372), channel_id=1, source_target_pairs={{0,6},{2,0},{4,2},{6,4},{1,7},{3,1},{5,3},{7,5},{8,14},{10,8},{12,... | collective-permute-start | bytes 393224 | tf_op jit(solution)/shard_map/ppermute | solution.py:17
  372.6 0.8 copy-start.6
  373.4 12.7 %collective-permute-start.13 = (bf16[32,2048]{0,1:T(8,128)(2,1)}, bf16[32,2048]{0,1:T(8,128)(2,1)S(1)}, u32[]{:S(2)}, u32[]{:S(2)}) collective-permute-start(bf16[32,2048]{0,1:T(8,128)(2,1)} %bitcast.158), channel_id=1, source_target_pairs={{0,2},{2,4},{4,6},{6,0},{1,3},{3,5},{5,7},{7,1},{8,10},{10,12},{12... | collective-permute-start | bytes 393224 | tf_op jit(solution)/shard_map/ppermute | solution.py:17
  386.7 5.4 collective-permute-start.15
  392.5 3.3 collective-permute-start.16
  479.9 1.3 copy-start.2
  481.3 8.9 %collective-permute-start.17 = (bf16[4,32,8,512]{3,2,1,0:T(8,128)(2,1)S(1)}, bf16[4,32,8,512]{3,2,1,0:T(8,128)(2,1)}, u32[]{:S(2)}, u32[]{:S(2)}) collective-permute-start(bf16[4,32,8,512]{3,2,1,0:T(8,128)(2,1)S(1)} %select_bitcast_fusion.3), channel_id=1, source_target_pairs={{0,1},{1,0},{2,3},{3,2},{4,5},{5,4},{6,7},{7,6},{8,9},{9,8},{10,11... | collective-permute-start | bytes 3145736 | tf_op jit(solution)/shard_map/ppermute | solution.py:17
  492.6 6.0 collective-permute-start.18
  493.9 4.7 collective-permute-start.20
  498.7 20.6 %collective-permute-start.19 = (bf16[32,8,512]{2,1,0:T(8,128)(2,1)S(1)}, bf16[32,8,512]{2,1,0:T(8,128)(2,1)}, u32[]{:S(2)}, u32[]{:S(2)}) collective-permute-start(bf16[32,8,512]{2,1,0:T(8,128)(2,1)S(1)} %pad_maximum_fusion.11), channel_id=1, source_target_pairs={{0,2},{2,4},{4,6},{6,0},{1,3},{3,5},{5,7},{7,1},{8,10},{10,12},{12... | collective-permute-start | bytes 786440 | tf_op jit(solution)/shard_map/ppermute | solution.py:17
  500.4 18.9 %collective-permute-start.21 = (bf16[32,8,512]{2,1,0:T(8,128)(2,1)}, bf16[32,8,512]{2,1,0:T(8,128)(2,1)}, u32[]{:S(2)}, u32[]{:S(2)}) collective-permute-start(bf16[32,8,512]{2,1,0:T(8,128)(2,1)} %pad_maximum_fusion.12), channel_id=1, source_target_pairs={{0,6},{2,0},{4,2},{6,4},{1,7},{3,1},{5,3},{7,5},{8,14},{10,8},{12,... | collective-permute-start | bytes 786440 | tf_op jit(solution)/shard_map/ppermute | solution.py:17
  647.3 6.4 collective-permute-start.22
  647.3 6.6 collective-permute-start.23
  653.8 5.6 collective-permute-start.24
  654.0 5.4 collective-permute-start.25
  659.5 8.4 %collective-permute-start.26 = (bf16[4,8,16384]{2,1,0:T(8,128)(2,1)S(1)}, bf16[4,8,16384]{2,1,0:T(8,128)(2,1)S(1)}, u32[]{:S(2)}, u32[]{:S(2)}) collective-permute-start(bf16[4,8,16384]{2,1,0:T(8,128)(2,1)S(1)} %fusion.76), channel_id=1, source_target_pairs={{0,1},{1,0},{2,3},{3,2},{4,5},{5,4},{6,7},{7,6},{8,9},{9,8},{10,11... | collective-permute-start | bytes 3145736 | tf_op jit(solution)/shard_map/ppermute | solution.py:17
  668.1 2.4 copy-start.1
